TPU v7x, 32 devices: a whole 2x2x4 slice. The times are simulated.
32 devices in a mesh: ep: 8 (over z, y), tp: 4 (over x, core).
Axes of the slice: x: 2, y: 2, z: 4, core: 2. Of those that a mesh axis runs over, the one named last changes fastest.
Arguments:
- tokens: bfloat16 [2048, 2048], P('ep', 'tp'), may hold values from -400 to 400
- expert_ids: int32 [2048, 2], P('ep'), may hold values from 0 to 7, all different within a row; in each aligned block of 256 rows (0 to 255, 256 to 511, ...) at most 80 rows name the same one
- route_weights: float32 [2048, 2], P('ep'), may hold values from 0.1 to 1
- pre_gain: float32 [2048], P('tp'), may hold values from 0.1 to 1.9
- post_gain: float32 [2048], P('tp'), may hold values from 0.1 to 1.9
- gate_weight: bfloat16 [8, 2048, 4096], P('ep', None, 'tp'), may hold values from -0.125 to 0.125
- up_weight: bfloat16 [8, 2048, 4096], P('ep', None, 'tp'), may hold values from -0.125 to 0.125
- down_weight: bfloat16 [8, 4096, 2048], P('ep', None, 'tp'), may hold values from -0.71875 to 0.71875
Outputs:
- layer_out: bfloat16 [2048, 2048], P('ep', 'tp')
Inputs may be any that keep to these rules, and one draw needn't show every extreme that they name: `expert_ids`: the 2 experts of a token are distinct. Within the rows of one device along ep, no expert is named more than 80 times, a bound that some block reaches.
All inputs are finite; a program needn't handle non-finite values.
Results may differ from a plain program's by a relative error of at most 0.007.
Values may be sent and summed in bfloat16 or wider, within the bound.
A program may use at most 64 MiB of HBM per device.

v0:
```python
import jax
import jax.numpy as jnp
from jax import lax
from jax.sharding import PartitionSpec as P

epsilon = 1e-06


def on_device(
    tokens, expert_ids, route_weights, pre_gain, post_gain, gate_weight, up_weight, down_weight
):
    tok_rows, width_part = tokens.shape
    width_full = width_part * lax.axis_size("tp")
    ep_count = lax.axis_size("ep")
    local_count = gate_weight.shape[0]
    experts_all = local_count * ep_count
    top_count = expert_ids.shape[1]
    capacity = max(2, tok_rows * top_count * 5 // (4 * experts_all))
    slot_total = experts_all * capacity
    tok_float = tokens.astype(jnp.float32)
    square_sum = lax.psum(jnp.sum(tok_float * tok_float, axis=1), "tp")
    inv_scale = lax.rsqrt(square_sum / width_full + epsilon)
    normed = (tok_float * inv_scale[:, None] * pre_gain[None, :]).astype(jnp.bfloat16)
    flat_ids = expert_ids.reshape(-1)
    onehot = (flat_ids[:, None] == jnp.arange(experts_all, dtype=jnp.int32)[None, :]).astype(
        jnp.int32
    )
    slot = jnp.sum((jnp.cumsum(onehot, axis=0) - 1) * onehot, axis=1)
    target = (flat_ids * capacity + slot).reshape(tok_rows, top_count)
    slot_index = jnp.arange(slot_total, dtype=jnp.int32)
    pick_map = (jnp.transpose(target).reshape(-1)[:, None] == slot_index[None, :]).astype(
        jnp.bfloat16
    )
    dispatch_map = jnp.sum(pick_map.reshape(top_count, tok_rows, slot_total), axis=0)
    outgoing = jnp.dot(
        jnp.transpose(dispatch_map), normed, preferred_element_type=jnp.float32
    ).astype(jnp.bfloat16)
    outgoing = outgoing.reshape(ep_count, local_count, capacity, width_part)
    arrived = lax.all_to_all(outgoing, "ep", split_axis=0, concat_axis=2, tiled=True)
    arrived = arrived.reshape(local_count, ep_count * capacity, width_part)
    row_total = ep_count * capacity
    features = lax.all_gather(arrived, "tp", axis=2, tiled=True)
    gate = jnp.einsum("erd,edh->erh", features, gate_weight, preferred_element_type=jnp.float32)
    upper = jnp.einsum("erd,edh->erh", features, up_weight, preferred_element_type=jnp.float32)
    hidden = (jax.nn.silu(gate) * upper).astype(jnp.bfloat16)
    hidden_whole = lax.all_gather(hidden, "tp", axis=2, tiled=True)
    result = jnp.einsum(
        "erh,ehd->erd", hidden_whole, down_weight, preferred_element_type=jnp.float32
    )
    expert_out = result.astype(jnp.bfloat16).reshape(1, local_count, row_total, width_part)
    returned = lax.all_to_all(expert_out, "ep", split_axis=2, concat_axis=0, tiled=True)
    returned = returned.reshape(slot_total, width_part)
    picked = jnp.dot(pick_map, returned, preferred_element_type=jnp.float32).reshape(
        top_count, tok_rows, width_part
    )
    mixed = jnp.sum(picked * jnp.transpose(route_weights)[:, :, None], axis=0)
    out_sum = lax.psum(jnp.sum(mixed * mixed, axis=1), "tp")
    out_scale = lax.rsqrt(out_sum / width_full + epsilon)
    return (mixed * out_scale[:, None] * post_gain[None, :]).astype(jnp.bfloat16)


def solution(mesh):
    return jax.shard_map(
        on_device,
        mesh=mesh,
        in_specs=(
            P("ep", "tp"),
            P("ep", None),
            P("ep", None),
            P("tp"),
            P("tp"),
            P("ep", None, "tp"),
            P("ep", None, "tp"),
            P("ep", None, "tp"),
        ),
        out_specs=P("ep", "tp"),
        check_vma=False,
    )
```

profile of v0, /device:TPU:0, one launch (start us, length us, event | category | flops | bytes accessed | tf_op | source)
XLA Modules:
  0.0 170.0 jit_solution(17323781832735627482)
XLA Ops:
  6.5 0.8 copy.39
  7.7 1.1 reduce-window.6
  8.8 0.2 slice_reduce_fusion
  9.2 0.1 reduce_sum.51
  9.4 0.7 add_bitcast_fusion
  10.1 0.2 fusion.24
  10.3 1.1 fusion.28
  11.4 8.4 %psum.14 = f32[256]{0:T(256)S(1)} all-reduce(f32[256]{0:T(256)S(1)} %fusion.28), channel_id=1, replica_groups=mesh['ep'=8,'tp'=4] {'tp'}, use_global_device_ids=true, to_apply=%region_5.6 | all-reduce | flops 256 | bytes 2048 | tf_op jit(solution)/shard_map/psum | solution.py:21
  19.7 1.4 convolution_convert_fusion
  21.1 22.2 %all_to_all.8 = bf16[8,1,80,512]{3,2,1,0:T(8,128)(2,1)} all-to-all(bf16[8,1,80,512]{3,2,1,0:T(8,128)(2,1)S(1)} %bitcast.53), channel_id=1, replica_groups=mesh['ep'=8,'tp'=4] {'ep'}, dimensions={0} | all-to-all | bytes 1310720 | tf_op jit(solution)/shard_map/all_to_all | solution.py:39
  43.4 24.3 %all-gather.4.cloned.1.call-done = bf16[1,640,2048]{2,1,0:T(8,128)(2,1)} async-done(((bf16[1,640,512]{2,1,0:T(8,128)(2,1)}), bf16[1,640,2048]{2,1,0:T(8,128)(2,1)}) %all-gather.4.cloned.1.call-update) | async-done | bytes 2621456 | tf_op jit(solution)/shard_map/all_gather | solution.py:42
  67.8 5.6 %fusion.4 = f32[640,1024]{1,0:T(8,128)S(1)} fusion(bf16[1,2048,1024]{2,1,0:T(8,128)(2,1)} %param.13, bf16[1,640,2048]{2,1,0:T(8,128)(2,1)} %all-gather.4.cloned.1.call-done), kind=kOutput, calls=%fused_computation.4 | convolution fusion | flops 2684354560 | bytes 9437184 | tf_op jit(solution)/shard_map/erd,edh->erh/dot_general | solution.py:43
  73.4 4.2 %multiply_convert_fusion = bf16[640,1024]{1,0:T(8,128)(2,1)} fusion(f32[640,1024]{1,0:T(8,128)S(1)} %fusion.4, bf16[1,2048,1024]{2,1,0:T(8,128)(2,1)S(1)} %copy-done.1, bf16[1,640,2048]{2,1,0:T(8,128)(2,1)S(1)} %copy-done.2), kind=kOutput, calls=%fused_computation.8 | convolution fusion | flops 2688286720 | bytes 10747904 | tf_op jit(solution)/shard_map/erd,edh->erh/dot_general | solution.py:44
  77.6 40.6 %all-gather.6.cloned.1.call-done = bf16[640,4096]{1,0:T(8,128)(2,1)} async-done(((bf16[640,1024]{1,0:T(8,128)(2,1)}), bf16[640,4096]{1,0:T(8,128)(2,1)}) %all-gather.6.cloned.1.call-update) | async-done | bytes 5242896 | tf_op jit(solution)/shard_map/all_gather | solution.py:46
  118.2 6.6 %fusion.21 = bf16[1,1,640,512]{3,2,1,0:T(8,128)(2,1)S(1)} fusion(bf16[640,4096]{1,0:T(8,128)(2,1)} %all-gather.6.cloned.1.call-done, bf16[1,4096,512]{2,1,0:T(8,128)(2,1)} %param.15), kind=kOutput, calls=%fused_computation.17 | convolution fusion | flops 2684682240 | bytes 10092544 | tf_op jit(solution)/shard_map/erh,ehd->erd/dot_general | solution.py:47
  124.8 1.0 copy.50
  125.8 0.5 broadcast.77
  126.3 4.8 %reduce.3 = bf16[640,512]{1,0:T(8,128)(2,1)S(1)} reduce(bf16[640,1,1,512]{3,2,1,0:T(2,128)(2,1)S(1)} %bitcast.51, bf16[]{:T(256)} %broadcast.77), dimensions={1,2}, to_apply=%bitcast.50.reduce_sub_computation | reduce | bytes 1310722
  131.1 0.5 reshape.125
  131.6 23.4 %all_to_all.9 = bf16[8,2,20480]{2,1,0:T(2,128)(2,1)S(1)} all-to-all(bf16[8,2,20480]{2,1,0:T(2,128)(2,1)S(1)} %reshape.125), channel_id=1, replica_groups=mesh['ep'=8,'tp'=4] {'ep'}, dimensions={0} | all-to-all | bytes 1310720 | tf_op jit(solution)/shard_map/all_to_all | solution.py:51
  155.0 0.6 reshape.126
  155.6 0.6 fusion.18
  156.4 6.0 %psum.15 = f32[256]{0:T(256)S(1)} all-reduce(f32[256]{0:T(256)S(1)} %multiply_reduce_fusion), channel_id=1, replica_groups=mesh['ep'=8,'tp'=4] {'tp'}, use_global_device_ids=true, to_apply=%region_8.9 | all-reduce | flops 256 | bytes 2048 | tf_op jit(solution)/shard_map/psum | solution.py:57
  162.4 0.8 multiply_convert_fusion.1
  (22 shorter events, 0.7 us)
Async XLA Ops:
  6.5 61.2 %all-gather.4.cloned.1.call-start = ((), (), s32[]{:S(2)}) async-start(), calls=%async_computation.2 | async-start | bytes 3276800 | tf_op jit(solution)/shard_map/all_gather | solution.py:42
  43.4 74.8 %all-gather.6.cloned.1.call-start = ((), (), s32[]{:S(2)}) async-start(), calls=%async_computation.3 | async-start | bytes 6553600 | tf_op jit(solution)/shard_map/all_gather | solution.py:46
  67.8 5.6 %copy-start.1 = (bf16[1,2048,1024]{2,1,0:T(8,128)(2,1)S(1)}, bf16[1,2048,1024]{2,1,0:T(8,128)(2,1)}, u32[]{:S(2)}) copy-start(bf16[1,2048,1024]{2,1,0:T(8,128)(2,1)} %param.14) | copy-start | bytes 12582916
  67.8 5.6 %copy-start.2 = (bf16[1,640,2048]{2,1,0:T(8,128)(2,1)S(1)}, bf16[1,640,2048]{2,1,0:T(8,128)(2,1)}, u32[]{:S(2)}) copy-start(bf16[1,640,2048]{2,1,0:T(8,128)(2,1)} %all-gather.4.cloned.1.call-done) | copy-start | bytes 7864324
  131.1 24.5 %copy-start.3 = (f32[256,2]{0,1:T(2,128)S(1)}, f32[256,2]{0,1:T(2,128)}, u32[]{:S(2)}) copy-start(f32[256,2]{0,1:T(2,128)} %param.10) | copy-start | bytes 6148
  155.0 7.4 %copy-start = (f32[512]{0:T(512)S(1)}, f32[512]{0:T(512)}, u32[]{:S(2)}) copy-start(f32[512]{0:T(512)} %param.12) | copy-start | bytes 6148
Sparse Core Ops, SparseCore 0:
  43.5 24.2 all-gather.3
  77.7 40.3 all-gather.5
where the time goes:
time: 170 us
  waiting for transfers between devices  64.9 us (38%)
  blocking collectives  59.9 us (35%)
  matrix products  18.4 us (11%)
  between operations  13.5 us (8%)
  other arithmetic  8.99 us (5%)
  local copies, waits for them, and re-layouts  4.19 us (2%)
    all_gather x1, waiting for transfers between devices, on_device(): hidden_whole = lax.all_gather(hidden, 'tp', axis=2, tiled=True)  40.6 us
    all_gather x1, waiting for transfers between devices, on_device(): features = lax.all_gather(arrived, 'tp', axis=2, tiled=True)  24.3 us
    all_to_all x1, blocking collectives, on_device(): lax.all_to_all(expert_out, 'ep', split_axis=2, concat_axis=0, tiled=True)  23.4 us
    all_to_all x1, blocking collectives, on_device(): lax.all_to_all(outgoing, 'ep', split_axis=0, concat_axis=2, tiled=True)  22.2 us
    psum x1, blocking collectives, on_device(): square_sum = lax.psum(jnp.sum(tok_float * tok_float, axis=1), 'tp')  8.37 us
    dot_general x1, matrix products, on_device(): jnp.einsum('erh,ehd->erd', hidden_whole, down_weight, preferred_element_t...  6.62 us
    psum x1, blocking collectives, on_device(): out_sum = lax.psum(jnp.sum(mixed * mixed, axis=1), 'tp')  5.95 us
    dot_general x1, matrix products, on_device(): jnp.einsum('erd,edh->erh', features, gate_weight, preferred_element_type=...  5.58 us
  transfers between devices with their start and end apart: 2, of which 2 were waited for; matrix products, arithmetic and copies ran while one was open for 0% of the time, Pallas kernels for 0%

commit v1 on v0

v1 whole, which is shorter than its diff:
```python
import functools

import jax
import jax.numpy as jnp
from jax import lax
from jax.experimental import pallas as pl
from jax.experimental.pallas import tpu as pltpu
from jax.sharding import PartitionSpec as P

epsilon = 1e-06
MESH = pl.DeviceIdType.MESH
f32, bf16 = jnp.float32, jnp.bfloat16


def flip(index, bits):
    out, bit = index, 1
    while bit <= bits:
        if bits & bit:
            out = out + bit * (1 - 2 * ((index // bit) % 2))
        bit *= 2
    return out


def to_column(row):
    return jnp.transpose(jnp.broadcast_to(row, (128, row.shape[1])))


def row_sums(values):
    part = values[:, 0:128]
    for at in range(128, values.shape[1], 128):
        part = part + values[:, at : at + 128]
    return jnp.sum(jnp.transpose(part), axis=0, keepdims=True)


def kernel(
    n, tp, capacity, cap, groups, order,
    tok_ref, ids_ref, rw_ref, pre_ref, post_ref, wg_hbm, wu_hbm, wd_hbm,
    out_ref,
    wg, wu, wd, outg, feats, hid, back, ret, pick, ss_in, ss_out,
    w_sem, si_s, si_r, so_s, so_r, d_s, d_r, fx_s, fx_r, fp_s, fp_r,
    hx_s, hx_r, hp_s, hp_r, r_s, r_r,
):
    me, ti = lax.axis_index("ep"), lax.axis_index("tp")
    chips = tp // 2
    chip, core = ti // 2, ti % 2
    partner = chip * 2 + (1 - core)
    rows, width = tok_ref.shape
    units = wg.shape[1]
    n_tile = min(256, units)
    tiles = units // n_tile
    per_group = n // groups
    group_rows = per_group * cap

    barrier = pltpu.get_barrier_semaphore()
    for d in range(1, n):
        pl.semaphore_signal(barrier, inc=1, device_id={"ep": flip(me, d)}, device_id_type=MESH)
    for j in range(1, tp):
        pl.semaphore_signal(barrier, inc=1, device_id={"tp": (ti + j) % tp}, device_id_type=MESH)
    loads = [
        pltpu.make_async_copy(src.at[0], dst, w_sem.at[i])
        for i, (src, dst) in enumerate(((wg_hbm, wg), (wu_hbm, wu), (wd_hbm, wd)))
    ]
    for load in loads:
        load.start()
    sent = []

    def remote(src, dst, s_sem, r_sem, where):
        return pltpu.make_async_remote_copy(
            src_ref=src, dst_ref=dst, send_sem=s_sem, recv_sem=r_sem,
            device_id=where, device_id_type=MESH,
        )

    def go(copy):
        copy.start()
        sent.append(copy)

    def total_over_tp(buf, s_sem, r_sem, row, before_wait=None):
        buf[0] = row
        if before_wait is not None:
            before_wait()
        copies = [
            remote(buf.at[0], buf.at[j], s_sem.at[j], r_sem.at[j], {"tp": (ti + j) % tp})
            for j in range(1, tp)
        ]
        for copy in copies:
            go(copy)
        return copies

    tok = tok_ref[...].astype(f32)
    square_row = row_sums(tok * tok)
    in_copies = total_over_tp(
        ss_in, si_s, si_r, square_row,
        lambda: pl.semaphore_wait(barrier, n - 1 + tp - 1),
    )

    lanes = max(n, 16)
    rel = [jnp.bitwise_xor(ids_ref[k : k + 1, :], me) for k in range(2)]
    d_iota = lax.broadcasted_iota(jnp.int32, (lanes, rows), 0)
    hot = [jnp.where(rel[k] == d_iota, 1.0, 0.0).astype(f32) for k in range(2)]
    earlier = jnp.where(
        lax.broadcasted_iota(jnp.int32, (rows, rows), 0)
        < lax.broadcasted_iota(jnp.int32, (rows, rows), 1), 1.0, 0.0,
    ).astype(bf16)
    prefix = jnp.dot((hot[0] + hot[1]).astype(bf16), earlier, preferred_element_type=f32)
    target = [
        rel[k].astype(f32) * cap + jnp.sum(prefix * hot[k], axis=0, keepdims=True)
        for k in range(2)
    ]
    slot_iota = lax.broadcasted_iota(jnp.int32, (cap, rows), 0).astype(f32)

    for copy in in_copies:
        copy.wait_recv()
    total = ss_in[0]
    for j in range(1, tp):
        total = total + ss_in[j]
    scale = to_column(lax.rsqrt(total / (width * tp) + epsilon))[:, 0:1]
    normed = (tok_ref[...].astype(f32) * scale * pre_ref[...]).astype(bf16)

    own = pl.ds(pl.multiple_of(ti * width, 128), width)

    def block(d):
        return pl.ds(d * cap, cap)

    def group(g):
        return pl.ds(g * group_rows, group_rows)

    def dispatch_copy(d):
        return remote(
            outg.at[block(d)], feats.at[block(d), own], d_s.at[d], d_r.at[d], {"ep": flip(me, d)}
        )

    def feat_x(g, j):
        ref = feats.at[group(g), own]
        where = {"tp": ((chip + j) % chips) * 2 + core}
        return remote(ref, ref, fx_s.at[g, j], fx_r.at[g, j], where)

    def feat_pair(g, j):
        source = ((chip + chips - j) % chips) * 2 + core
        ref = feats.at[group(g), pl.ds(pl.multiple_of(source * width, 128), width)]
        return remote(ref, ref, fp_s.at[g, j], fp_r.at[g, j], {"tp": partner})

    def share(g):
        for j in range(1, chips):
            go(feat_x(g, j))
        go(feat_pair(g, 0))

    def pass_on(g):
        for j in range(1, chips):
            feat_x(g, j).wait_recv()
            go(feat_pair(g, j))

    for d in range(n):
        base = float(d * cap)
        chosen = jnp.where(
            (target[0] == slot_iota + base) | (target[1] == slot_iota + base), 1.0, 0.0
        ).astype(bf16)
        picked = jnp.dot(chosen, normed, preferred_element_type=f32).astype(bf16)
        if d == 0:
            feats[block(0), own] = picked
        else:
            outg[block(d), :] = picked
            go(dispatch_copy(d))
        if d == per_group - 1 and per_group == 1:
            share(0)

    lane = lax.broadcasted_iota(jnp.int32, (rows, 128), 1).astype(f32)
    for k in range(2):
        column = to_column(target[k])
        for at in range(0, n * cap, 128):
            pick[k, :, at : at + 128] = jnp.where(column == lane + float(at), 1.0, 0.0).astype(bf16)

    chunk_groups = groups // len(order)

    def hid_ref(q, owner, i):
        at = pl.multiple_of(owner * units + i * n_tile, 128)
        return hid.at[pl.ds(q * chunk_groups * group_rows, chunk_groups * group_rows), pl.ds(at, n_tile)]

    def hid_x(q, i, j):
        ref = hid_ref(q, ti, i)
        where = {"tp": ((chip + j) % chips) * 2 + core}
        return remote(ref, ref, hx_s.at[q, i, j], hx_r.at[q, i, j], where)

    def hid_pair(q, i, j):
        ref = hid_ref(q, ((chip + chips - j) % chips) * 2 + core, i)
        return remote(ref, ref, hp_s.at[q, i, j], hp_r.at[q, i, j], {"tp": partner})

    def chunk(q):
        return pl.ds(q * chunk_groups * group_rows, chunk_groups * group_rows)

    def gate_up(q):
        for g in range(q * chunk_groups, (q + 1) * chunk_groups):
            for j in range(chips):
                feat_pair(g, j).wait_recv()

        def tile(i, carry):
            cols = pl.ds(pl.multiple_of(i * n_tile, 128), n_tile)
            x = feats[chunk(q), :]
            gate = jnp.dot(x, wg[:, cols], preferred_element_type=f32)
            upper = jnp.dot(x, wu[:, cols], preferred_element_type=f32)
            value = gate / (1.0 + jnp.exp(-gate)) * upper
            mine = pl.ds(pl.multiple_of(ti * units + i * n_tile, 128), n_tile)
            hid[chunk(q), mine] = value.astype(bf16)
            for j in range(1, chips):
                hid_x(q, i, j).start()
            hid_pair(q, i, 0).start()
            return carry

        lax.fori_loop(0, tiles, tile, 0)

    ready = {q: (q + 1) * chunk_groups - 1 for q in range(len(order))}
    state = {"done": 0, "weights": False}

    def advance(upto):
        while state["done"] < len(order) and max(
            ready[q] for q in order[: state["done"] + 1]
        ) <= upto:
            if not state["weights"]:
                loads[0].wait()
                loads[1].wait()
                state["weights"] = True
            gate_up(order[state["done"]])
            state["done"] += 1

    for g in range(groups):
        for d in range(g * per_group, (g + 1) * per_group):
            if d > 0:
                dispatch_copy(d).wait_recv()
        if not (g == 0 and per_group == 1):
            share(g)
        if g > 0:
            pass_on(g - 1)
            advance(g - 2)
    pass_on(groups - 1)
    advance(groups - 1)

    out_tile = min(256, width)

    def return_copy(d):
        return remote(back.at[block(d)], ret.at[block(d)], r_s.at[d], r_r.at[d], {"ep": flip(me, d)})

    loads[2].wait()
    for q in order:
        def relay(i, carry):
            for j in range(1, chips):
                hid_x(q, i, j).wait_recv()
                hid_pair(q, i, j).start()
            return carry

        def arrive(i, carry):
            for j in range(chips):
                hid_pair(q, i, j).wait_recv()
            return carry

        lax.fori_loop(0, tiles, relay, 0)
        lax.fori_loop(0, tiles, arrive, 0)

        def down(i, carry):
            cols = pl.ds(pl.multiple_of(i * out_tile, 128), out_tile)
            back[chunk(q), cols] = jnp.dot(
                hid[chunk(q), :], wd[:, cols], preferred_element_type=f32
            ).astype(bf16)
            return carry

        lax.fori_loop(0, width // out_tile, down, 0)
        first = q * chunk_groups * per_group
        for d in range(first, first + chunk_groups * per_group):
            if d > 0:
                go(return_copy(d))
    ret[block(0), :] = back[block(0), :]
    for d in range(1, n):
        return_copy(d).wait_recv()

    mixed = 0.0
    for k in range(2):
        picked = jnp.dot(pick[k], ret[...], preferred_element_type=f32)
        mixed = mixed + picked * to_column(rw_ref[k : k + 1, :])[:, 0:1]
    out_copies = total_over_tp(ss_out, so_s, so_r, row_sums(mixed * mixed))
    for copy in sent[: -len(out_copies)]:
        copy.wait_send()
    for q in order:
        def drain(i, carry):
            for j in range(1, chips):
                hid_x(q, i, j).wait_send()
            for j in range(chips):
                hid_pair(q, i, j).wait_send()
            return carry

        lax.fori_loop(0, tiles, drain, 0)
    for copy in out_copies:
        copy.wait_recv()
    total = ss_out[0]
    for j in range(1, tp):
        total = total + ss_out[j]
    scale = to_column(lax.rsqrt(total / (width * tp) + epsilon))[:, 0:1]
    out_ref[...] = (mixed * scale * post_ref[...]).astype(bf16)
    for copy in out_copies:
        copy.wait_send()


def on_device(
    tokens, expert_ids, route_weights, pre_gain, post_gain, gate_weight, up_weight, down_weight
):
    rows, width = tokens.shape
    n, tp = lax.axis_size("ep"), lax.axis_size("tp")
    assert gate_weight.shape[0] == 1 and expert_ids.shape[1] == 2
    capacity = max(2, rows * 2 * 5 // (4 * n))
    cap = -(-capacity // 16) * 16
    groups = min(8, n)
    order = (1, 2, 3, 0)
    slots = n * cap
    chips = tp // 2
    features, units = gate_weight.shape[1:]
    hidden_all = units * tp
    tiles = units // min(256, units)
    chunks = len(order)
    dma = pltpu.SemaphoreType.DMA
    vmem = pl.BlockSpec(memory_space=pltpu.VMEM)
    hbm = pl.BlockSpec(memory_space=pl.ANY)
    return pl.pallas_call(
        functools.partial(kernel, n, tp, capacity, cap, groups, order),
        out_shape=jax.ShapeDtypeStruct((rows, width), bf16),
        in_specs=[vmem] * 5 + [hbm] * 3,
        out_specs=vmem,
        scratch_shapes=[
            pltpu.VMEM((features, units), bf16),
            pltpu.VMEM((features, units), bf16),
            pltpu.VMEM((hidden_all, width), bf16),
            pltpu.VMEM((slots, width), bf16),
            pltpu.VMEM((slots, features), bf16),
            pltpu.VMEM((slots, hidden_all), bf16),
            pltpu.VMEM((slots, width), bf16),
            pltpu.VMEM((slots, width), bf16),
            pltpu.VMEM((2, rows, slots), bf16),
            pltpu.VMEM((tp, 1, rows), f32),
            pltpu.VMEM((tp, 1, rows), f32),
            dma((3,)),
            dma((tp,)), dma((tp,)), dma((tp,)), dma((tp,)),
            dma((n,)), dma((n,)),
            dma((groups, chips)), dma((groups, chips)),
            dma((groups, chips)), dma((groups, chips)),
            dma((chunks, tiles, chips)), dma((chunks, tiles, chips)),
            dma((chunks, tiles, chips)), dma((chunks, tiles, chips)),
            dma((n,)), dma((n,)),
        ],
        compiler_params=pltpu.CompilerParams(
            collective_id=0, has_side_effects=True, vmem_limit_bytes=56 * 1024 * 1024
        ),
    )(
        tokens, jnp.transpose(expert_ids), jnp.transpose(route_weights),
        pre_gain.reshape(1, -1), post_gain.reshape(1, -1),
        gate_weight, up_weight, down_weight,
    )


def solution(mesh):
    return jax.shard_map(
        on_device,
        mesh=mesh,
        in_specs=(
            P("ep", "tp"),
            P("ep", None),
            P("ep", None),
            P("tp"),
            P("tp"),
            P("ep", None, "tp"),
            P("ep", None, "tp"),
            P("ep", None, "tp"),
        ),
        out_specs=P("ep", "tp"),
        check_vma=False,
    )
```

time: 170 us -> 71.8 us (0.42)
  Pallas kernels: 0 us -> 69.9 us
  waiting for transfers between devices: 64.9 us -> 0 us
  blocking collectives: 59.9 us -> 0 us
  matrix products: 18.4 us -> 0 us
  between operations: 13.5 us -> 0.01 us
  other arithmetic: 8.99 us -> 0 us
  local copies, waits for them, and re-layouts: 4.19 us -> 1.67 us
    pallas_call x0 -> x1, Pallas kernels: none -> 69.9 us  [on_device(): pl.pallas_call(functools.partial(kernel, n, tp, capacity, cap, groups, or...]
    all_gather x2 -> x0, waiting for transfers between devices: 64.9 us -> none  [the longest x1 40.6 us: on_device(): hidden_whole = lax.all_gather(hidden, 'tp', axis=2, tiled=True)]
    all_to_all x2 -> x0, blocking collectives: 45.6 us -> none  [the longest x1 23.4 us: on_device(): lax.all_to_all(expert_out, 'ep', split_axis=2, concat_axis=0, tiled=True)]
    dot_general x5 -> x0, matrix products: 18.4 us -> none  [the longest x1 6.62 us: on_device(): jnp.einsum('erh,ehd->erd', hidden_whole, down_weight, preferred_element_t...]
    psum x2 -> x0, blocking collectives: 14.3 us -> none  [the longest x1 8.37 us: on_device(): square_sum = lax.psum(jnp.sum(tok_float * tok_float, axis=1), 'tp')]
    unnamed x1 -> x0, other arithmetic: 4.79 us -> none
  transfers between devices with their start and end apart: 2 -> 0, of which waited for: 2 -> 0; matrix products, arithmetic and copies ran while one was open for 0% -> 0% of each run, Pallas kernels for 0% -> 0%
where the time goes in v1:
time: 71.8 us; the launch traced here: 71.6 us
  Pallas kernels  69.9 us (97%)
  local copies, waits for them, and re-layouts  1.67 us (2%)
    pallas_call x1, Pallas kernels, on_device(): pl.pallas_call(functools.partial(kernel, n, tp, capacity, cap, groups, or...  69.9 us
    unnamed x1, local copies, waits for them, and re-layouts  1.67 us

profile of v1, /device:TPU:0, one launch (start us, length us, event | category | flops | bytes accessed | tf_op | source)
XLA Modules:
  0.0 71.6 jit_solution(15548834143814363869)
XLA Ops:
  0.0 69.9 %shard_map.82 = bf16[256,512]{1,0:T(8,128)(2,1)} custom-call(bf16[256,512]{1,0:T(8,128)(2,1)} %tok_ref.1, s32[2,256]{1,0:T(2,128)} %bitcast.4, f32[2,256]{1,0:T(2,128)} %bitcast.5, f32[1,512]{1,0:T(1,128)} %bitcast.6, f32[1,512]{1,0:T(1,128)} %bitcast.7, bf16[1,2048,1024]{2,1,0:T(8,128)(2,1)} %wg_hbm.1, bf16[1,2048,1024]{2,1,0:T(8,128)(2,1)} %wu_hbm.1, ...), custom_call_target="tpu_custom_call" | custom-call | tf_op jit(solution)/shard_map/pallas_call | solution.py:319
  69.9 1.7 %copy.10 = bf16[256,512]{1,0:T(8,128)(2,1)} copy(bf16[256,512]{1,0:T(8,128)(2,1)} %shard_map.82) | data formatting | bytes 524288

commit v2 on v1

--- a/solution.py
+++ b/solution.py
@@ -25,6 +25,10 @@
     return jnp.transpose(jnp.broadcast_to(row, (128, row.shape[1])))
 
 
+def wide(column, width):
+    return jnp.concatenate([column] * (width // 128), axis=1)
+
+
 def row_sums(values):
     part = values[:, 0:128]
     for at in range(128, values.shape[1], 128):
@@ -33,13 +37,14 @@
 
 
 def kernel(
-    n, tp, capacity, cap, groups, order,
+    n, tp, cap, groups, chunks, pieces,
     tok_ref, ids_ref, rw_ref, pre_ref, post_ref, wg_hbm, wu_hbm, wd_hbm,
     out_ref,
-    wg, wu, wd, outg, feats, hid, back, ret, pick, ss_in, ss_out,
-    w_sem, si_s, si_r, so_s, so_r, d_s, d_r, fx_s, fx_r, fp_s, fp_r,
-    hx_s, hx_r, hp_s, hp_r, r_s, r_r,
+    wg, wu, wd, outg, feats, rows_in, hid, back, ret, gain, ss_out, mix, wcol, *rest,
 ):
+    picks, sems = rest[: len(pieces)], rest[len(pieces) :]
+    (w_sem, g_s, g_r, so_s, so_r, d_s, d_r, fx_s, fx_r, fp_s, fp_r,
+     hx_s, hx_r, hp_s, hp_r, r_s, r_r) = sems
     me, ti = lax.axis_index("ep"), lax.axis_index("tp")
     chips = tp // 2
     chip, core = ti // 2, ti % 2
@@ -73,25 +78,6 @@
     def go(copy):
         copy.start()
         sent.append(copy)
-
-    def total_over_tp(buf, s_sem, r_sem, row, before_wait=None):
-        buf[0] = row
-        if before_wait is not None:
-            before_wait()
-        copies = [
-            remote(buf.at[0], buf.at[j], s_sem.at[j], r_sem.at[j], {"tp": (ti + j) % tp})
-            for j in range(1, tp)
-        ]
-        for copy in copies:
-            go(copy)
-        return copies
-
-    tok = tok_ref[...].astype(f32)
-    square_row = row_sums(tok * tok)
-    in_copies = total_over_tp(
-        ss_in, si_s, si_r, square_row,
-        lambda: pl.semaphore_wait(barrier, n - 1 + tp - 1),
-    )
 
     lanes = max(n, 16)
     rel = [jnp.bitwise_xor(ids_ref[k : k + 1, :], me) for k in range(2)]
@@ -108,14 +94,7 @@
     ]
     slot_iota = lax.broadcasted_iota(jnp.int32, (cap, rows), 0).astype(f32)
 
-    for copy in in_copies:
-        copy.wait_recv()
-    total = ss_in[0]
-    for j in range(1, tp):
-        total = total + ss_in[j]
-    scale = to_column(lax.rsqrt(total / (width * tp) + epsilon))[:, 0:1]
-    normed = (tok_ref[...].astype(f32) * scale * pre_ref[...]).astype(bf16)
-
+    tokens = tok_ref[...]
     own = pl.ds(pl.multiple_of(ti * width, 128), width)
 
     def block(d):
@@ -154,26 +133,52 @@
         chosen = jnp.where(
             (target[0] == slot_iota + base) | (target[1] == slot_iota + base), 1.0, 0.0
         ).astype(bf16)
-        picked = jnp.dot(chosen, normed, preferred_element_type=f32).astype(bf16)
+        picked = jnp.dot(chosen, tokens, preferred_element_type=f32).astype(bf16)
         if d == 0:
             feats[block(0), own] = picked
         else:
             outg[block(d), :] = picked
-            go(dispatch_copy(d))
-        if d == per_group - 1 and per_group == 1:
-            share(0)
-
-    lane = lax.broadcasted_iota(jnp.int32, (rows, 128), 1).astype(f32)
+    pl.semaphore_wait(barrier, n - 1 + tp - 1)
+    if per_group == 1:
+        share(0)
+    for d in range(1, n):
+        go(dispatch_copy(d))
+    gain[:, own] = pre_ref[...]
+
+    def gain_copy(j):
+        return remote(pre_ref, gain.at[:, own], g_s.at[j], g_r.at[j], {"tp": (ti + j) % tp})
+
+    for j in range(1, tp):
+        go(gain_copy(j))
+
+    def piece_slots(piece):
+        return pl.ds(piece[0] * group_rows, piece[1] * group_rows)
+
     for k in range(2):
         column = to_column(target[k])
-        for at in range(0, n * cap, 128):
-            pick[k, :, at : at + 128] = jnp.where(column == lane + float(at), 1.0, 0.0).astype(bf16)
-
-    chunk_groups = groups // len(order)
+        wcol[k] = to_column(rw_ref[k : k + 1, :])
+        for piece, pick in zip(pieces, picks):
+            base = piece[0] * group_rows
+            for at in range(0, pick.shape[2], 128):
+                size = min(128, pick.shape[2] - at)
+                lane = lax.broadcasted_iota(jnp.int32, (rows, size), 1).astype(f32)
+                pick[k, :, at : at + size] = jnp.where(
+                    column[:, 0:size] == lane + float(base + at), 1.0, 0.0
+                ).astype(bf16)
+
+    def combine(piece, pick, first):
+        value = 0.0 if first else mix[...]
+        for k in range(2):
+            found = jnp.dot(pick[k], ret[piece_slots(piece), :], preferred_element_type=f32)
+            value = value + found * wide(wcol[k], width)
+        return value
+
+    def chunk(q):
+        return pl.ds(chunks[q][0] * group_rows, chunks[q][1] * group_rows)
 
     def hid_ref(q, owner, i):
         at = pl.multiple_of(owner * units + i * n_tile, 128)
-        return hid.at[pl.ds(q * chunk_groups * group_rows, chunk_groups * group_rows), pl.ds(at, n_tile)]
+        return hid.at[chunk(q), pl.ds(at, n_tile)]
 
     def hid_x(q, i, j):
         ref = hid_ref(q, ti, i)
@@ -184,62 +189,66 @@
         ref = hid_ref(q, ((chip + chips - j) % chips) * 2 + core, i)
         return remote(ref, ref, hp_s.at[q, i, j], hp_r.at[q, i, j], {"tp": partner})
 
-    def chunk(q):
-        return pl.ds(q * chunk_groups * group_rows, chunk_groups * group_rows)
-
-    def gate_up(q):
-        for g in range(q * chunk_groups, (q + 1) * chunk_groups):
+    def send_tile(q, i):
+        for j in range(1, chips):
+            hid_x(q, i, j).start()
+        hid_pair(q, i, 0).start()
+
+    def send_hidden(q):
+        def body(i, carry):
+            send_tile(q, i)
+            return carry
+
+        lax.fori_loop(0, tiles, body, 0)
+
+    def gate_up(first, many, q=None):
+        for g in range(first, first + many):
             for j in range(chips):
                 feat_pair(g, j).wait_recv()
 
+        at, count = first * group_rows, many * group_rows
+        span = pl.ds(at, count)
+        batch = max(u for u in range(1, 6) if (count // 16) % u == 0)
+
+        def norm(i, carry):
+            for u in range(batch):
+                here = (i * batch + u) * 16
+                part = pl.ds(pl.multiple_of(at + here, 16), 16)
+                x = feats[part, :].astype(f32)
+                square = jnp.sum(x * x, axis=1, keepdims=True)
+                x = x * lax.rsqrt(square / (width * tp) + epsilon) * gain[...]
+                rows_in[pl.ds(pl.multiple_of(here, 16), 16), :] = x.astype(bf16)
+            return carry
+
+        lax.fori_loop(0, count // (16 * batch), norm, 0)
+
         def tile(i, carry):
             cols = pl.ds(pl.multiple_of(i * n_tile, 128), n_tile)
-            x = feats[chunk(q), :]
+            x = rows_in[0:count, :]
             gate = jnp.dot(x, wg[:, cols], preferred_element_type=f32)
             upper = jnp.dot(x, wu[:, cols], preferred_element_type=f32)
             value = gate / (1.0 + jnp.exp(-gate)) * upper
             mine = pl.ds(pl.multiple_of(ti * units + i * n_tile, 128), n_tile)
-            hid[chunk(q), mine] = value.astype(bf16)
-            for j in range(1, chips):
-                hid_x(q, i, j).start()
-            hid_pair(q, i, 0).start()
+            hid[span, mine] = value.astype(bf16)
+            if q is not None:
+                send_tile(q, i)
             return carry
 
         lax.fori_loop(0, tiles, tile, 0)
 
-    ready = {q: (q + 1) * chunk_groups - 1 for q in range(len(order))}
-    state = {"done": 0, "weights": False}
-
-    def advance(upto):
-        while state["done"] < len(order) and max(
-            ready[q] for q in order[: state["done"] + 1]
-        ) <= upto:
-            if not state["weights"]:
-                loads[0].wait()
-                loads[1].wait()
-                state["weights"] = True
-            gate_up(order[state["done"]])
-            state["done"] += 1
-
-    for g in range(groups):
+    def take(g):
         for d in range(g * per_group, (g + 1) * per_group):
             if d > 0:
                 dispatch_copy(d).wait_recv()
         if not (g == 0 and per_group == 1):
             share(g)
-        if g > 0:
-            pass_on(g - 1)
-            advance(g - 2)
-    pass_on(groups - 1)
-    advance(groups - 1)
 
     out_tile = min(256, width)
 
     def return_copy(d):
         return remote(back.at[block(d)], ret.at[block(d)], r_s.at[d], r_r.at[d], {"ep": flip(me, d)})
 
-    loads[2].wait()
-    for q in order:
+    def finish(q):
         def relay(i, carry):
             for j in range(1, chips):
                 hid_x(q, i, j).wait_recv()
@@ -262,22 +271,59 @@
             return carry
 
         lax.fori_loop(0, width // out_tile, down, 0)
-        first = q * chunk_groups * per_group
-        for d in range(first, first + chunk_groups * per_group):
+        for d in range(chunks[q][0] * per_group, sum(chunks[q]) * per_group):
             if d > 0:
                 go(return_copy(d))
-    ret[block(0), :] = back[block(0), :]
-    for d in range(1, n):
+        if chunks[q][0] == 0:
+            ret[block(0), :] = back[block(0), :]
+
+    take(0)
+    for g in range(1, 6):
+        take(g)
+        if g > 1:
+            pass_on(g - 2)
+    loads[0].wait()
+    loads[1].wait()
+    for j in range(1, tp):
+        gain_copy(j).wait_recv()
+    gate_up(2, 2, 0)
+    pass_on(4)
+    take(6)
+    take(7)
+    pass_on(5)
+    gate_up(4, 2, 1)
+    gate_up(0, 2)
+    loads[2].wait()
+    finish(0)
+    pass_on(6)
+    pass_on(7)
+    gate_up(6, 2, 2)
+    send_hidden(3)
+    send_hidden(4)
+    finish(1)
+    finish(2)
+    finish(3)
+    piece = pieces[0]
+    for d in range(piece[0] * per_group, sum(piece) * per_group):
         return_copy(d).wait_recv()
-
-    mixed = 0.0
-    for k in range(2):
-        picked = jnp.dot(pick[k], ret[...], preferred_element_type=f32)
-        mixed = mixed + picked * to_column(rw_ref[k : k + 1, :])[:, 0:1]
-    out_copies = total_over_tp(ss_out, so_s, so_r, row_sums(mixed * mixed))
-    for copy in sent[: -len(out_copies)]:
+    mix[...] = combine(piece, picks[0], True)
+    finish(4)
+    for piece, pick in zip(pieces[1:], picks[1:]):
+        for d in range(piece[0] * per_group, sum(piece) * per_group):
+            if d > 0:
+                return_copy(d).wait_recv()
+        mix[...] = combine(piece, pick, False)
+    mixed = mix[...]
+    ss_out[0] = row_sums(mixed * mixed)
+    out_copies = [
+        remote(ss_out.at[0], ss_out.at[j], so_s.at[j], so_r.at[j], {"tp": (ti + j) % tp})
+        for j in range(1, tp)
+    ]
+    for copy in out_copies:
+        copy.start()
+    for copy in sent:
         copy.wait_send()
-    for q in order:
+    for q in range(len(chunks)):
         def drain(i, carry):
             for j in range(1, chips):
                 hid_x(q, i, j).wait_send()
@@ -291,7 +337,7 @@
     total = ss_out[0]
     for j in range(1, tp):
         total = total + ss_out[j]
-    scale = to_column(lax.rsqrt(total / (width * tp) + epsilon))[:, 0:1]
+    scale = wide(to_column(lax.rsqrt(total / (width * tp) + epsilon)), width)
     out_ref[...] = (mixed * scale * post_ref[...]).astype(bf16)
     for copy in out_copies:
         copy.wait_send()
@@ -305,19 +351,22 @@
     assert gate_weight.shape[0] == 1 and expert_ids.shape[1] == 2
     capacity = max(2, rows * 2 * 5 // (4 * n))
     cap = -(-capacity // 16) * 16
-    groups = min(8, n)
-    order = (1, 2, 3, 0)
+    groups = 8
+    assert n % groups == 0
+    chunks = ((2, 2), (4, 2), (6, 2), (1, 1), (0, 1))
+    pieces = ((2, 4), (6, 2), (0, 2))
     slots = n * cap
     chips = tp // 2
     features, units = gate_weight.shape[1:]
     hidden_all = units * tp
     tiles = units // min(256, units)
-    chunks = len(order)
+    steps = len(chunks)
+    most = max(count for _, count in chunks) * (slots // groups)
     dma = pltpu.SemaphoreType.DMA
     vmem = pl.BlockSpec(memory_space=pltpu.VMEM)
     hbm = pl.BlockSpec(memory_space=pl.ANY)
     return pl.pallas_call(
-        functools.partial(kernel, n, tp, capacity, cap, groups, order),
+        functools.partial(kernel, n, tp, cap, groups, chunks, pieces),
         out_shape=jax.ShapeDtypeStruct((rows, width), bf16),
         in_specs=[vmem] * 5 + [hbm] * 3,
         out_specs=vmem,
@@ -327,19 +376,22 @@
             pltpu.VMEM((hidden_all, width), bf16),
             pltpu.VMEM((slots, width), bf16),
             pltpu.VMEM((slots, features), bf16),
+            pltpu.VMEM((most, features), bf16),
             pltpu.VMEM((slots, hidden_all), bf16),
             pltpu.VMEM((slots, width), bf16),
             pltpu.VMEM((slots, width), bf16),
-            pltpu.VMEM((2, rows, slots), bf16),
+            pltpu.VMEM((1, features), f32),
             pltpu.VMEM((tp, 1, rows), f32),
-            pltpu.VMEM((tp, 1, rows), f32),
+            pltpu.VMEM((rows, width), f32),
+            pltpu.VMEM((2, rows, 128), f32),
+            *[pltpu.VMEM((2, rows, count * (slots // groups)), bf16) for _, count in pieces],
             dma((3,)),
             dma((tp,)), dma((tp,)), dma((tp,)), dma((tp,)),
             dma((n,)), dma((n,)),
             dma((groups, chips)), dma((groups, chips)),
             dma((groups, chips)), dma((groups, chips)),
-            dma((chunks, tiles, chips)), dma((chunks, tiles, chips)),
-            dma((chunks, tiles, chips)), dma((chunks, tiles, chips)),
+            dma((steps, tiles, chips)), dma((steps, tiles, chips)),
+            dma((steps, tiles, chips)), dma((steps, tiles, chips)),
             dma((n,)), dma((n,)),
         ],
         compiler_params=pltpu.CompilerParams(

time: 71.8 us -> 66.3 us (0.923)
  Pallas kernels: 69.9 us -> 64.5 us
    pallas_call x1, Pallas kernels: 69.9 us -> 64.5 us  [on_device(): pl.pallas_call(functools.partial(kernel, n, tp, cap, groups, chunks, piec...]
where the time goes in v2:
time: 66.3 us; the launch traced here: 66.2 us
  Pallas kernels  64.5 us (97%)
  local copies, waits for them, and re-layouts  1.67 us (3%)
    pallas_call x1, Pallas kernels, on_device(): pl.pallas_call(functools.partial(kernel, n, tp, cap, groups, chunks, piec...  64.5 us
    unnamed x1, local copies, waits for them, and re-layouts  1.67 us

profile of v2, /device:TPU:0, one launch (start us, length us, event | category | flops | bytes accessed | tf_op | source)
XLA Modules:
  0.0 66.2 jit_solution(7814836626530017742)
XLA Ops:
  0.0 64.5 %shard_map.82 = bf16[256,512]{1,0:T(8,128)(2,1)} custom-call(bf16[256,512]{1,0:T(8,128)(2,1)} %tok_ref.1, s32[2,256]{1,0:T(2,128)} %bitcast.4, f32[2,256]{1,0:T(2,128)} %bitcast.5, f32[1,512]{1,0:T(1,128)} %bitcast.6, f32[1,512]{1,0:T(1,128)} %bitcast.7, bf16[1,2048,1024]{2,1,0:T(8,128)(2,1)} %wg_hbm.1, bf16[1,2048,1024]{2,1,0:T(8,128)(2,1)} %wu_hbm.1, ...), custom_call_target="tpu_custom_call" | custom-call | tf_op jit(solution)/shard_map/pallas_call | solution.py:368
  64.5 1.7 %copy.10 = bf16[256,512]{1,0:T(8,128)(2,1)} copy(bf16[256,512]{1,0:T(8,128)(2,1)} %shard_map.82) | data formatting | bytes 524288

commit v3 on v2

--- a/solution.py
+++ b/solution.py
@@ -67,7 +67,6 @@
     ]
     for load in loads:
         load.start()
-    sent = []
 
     def remote(src, dst, s_sem, r_sem, where):
         return pltpu.make_async_remote_copy(
@@ -77,7 +76,6 @@
 
     def go(copy):
         copy.start()
-        sent.append(copy)
 
     lanes = max(n, 16)
     rel = [jnp.bitwise_xor(ids_ref[k : k + 1, :], me) for k in range(2)]
@@ -105,18 +103,18 @@
 
     def dispatch_copy(d):
         return remote(
-            outg.at[block(d)], feats.at[block(d), own], d_s.at[d], d_r.at[d], {"ep": flip(me, d)}
+            outg.at[block(d)], feats.at[block(d), own], d_s.at[0], d_r.at[d - 1], {"ep": flip(me, d)}
         )
 
     def feat_x(g, j):
         ref = feats.at[group(g), own]
         where = {"tp": ((chip + j) % chips) * 2 + core}
-        return remote(ref, ref, fx_s.at[g, j], fx_r.at[g, j], where)
+        return remote(ref, ref, fx_s.at[0], fx_r.at[g, j - 1], where)
 
     def feat_pair(g, j):
         source = ((chip + chips - j) % chips) * 2 + core
         ref = feats.at[group(g), pl.ds(pl.multiple_of(source * width, 128), width)]
-        return remote(ref, ref, fp_s.at[g, j], fp_r.at[g, j], {"tp": partner})
+        return remote(ref, ref, fp_s.at[0], fp_r.at[g], {"tp": partner})
 
     def share(g):
         for j in range(1, chips):
@@ -146,7 +144,7 @@
     gain[:, own] = pre_ref[...]
 
     def gain_copy(j):
-        return remote(pre_ref, gain.at[:, own], g_s.at[j], g_r.at[j], {"tp": (ti + j) % tp})
+        return remote(pre_ref, gain.at[:, own], g_s.at[0], g_r.at[j - 1], {"tp": (ti + j) % tp})
 
     for j in range(1, tp):
         go(gain_copy(j))
@@ -183,11 +181,11 @@
     def hid_x(q, i, j):
         ref = hid_ref(q, ti, i)
         where = {"tp": ((chip + j) % chips) * 2 + core}
-        return remote(ref, ref, hx_s.at[q, i, j], hx_r.at[q, i, j], where)
+        return remote(ref, ref, hx_s.at[0], hx_r.at[q, i, j - 1], where)
 
     def hid_pair(q, i, j):
         ref = hid_ref(q, ((chip + chips - j) % chips) * 2 + core, i)
-        return remote(ref, ref, hp_s.at[q, i, j], hp_r.at[q, i, j], {"tp": partner})
+        return remote(ref, ref, hp_s.at[0], hp_r.at[q], {"tp": partner})
 
     def send_tile(q, i):
         for j in range(1, chips):
@@ -203,8 +201,8 @@
 
     def gate_up(first, many, q=None):
         for g in range(first, first + many):
-            for j in range(chips):
-                feat_pair(g, j).wait_recv()
+            ref = feats.at[group(g), 0 : chips * width]
+            remote(ref, ref, fp_s.at[0], fp_r.at[g], {"tp": partner}).wait_recv()
 
         at, count = first * group_rows, many * group_rows
         span = pl.ds(at, count)
@@ -246,7 +244,7 @@
     out_tile = min(256, width)
 
     def return_copy(d):
-        return remote(back.at[block(d)], ret.at[block(d)], r_s.at[d], r_r.at[d], {"ep": flip(me, d)})
+        return remote(back.at[block(d)], ret.at[block(d)], r_s.at[0], r_r.at[d - 1], {"ep": flip(me, d)})
 
     def finish(q):
         def relay(i, carry):
@@ -255,13 +253,9 @@
                 hid_pair(q, i, j).start()
             return carry
 
-        def arrive(i, carry):
-            for j in range(chips):
-                hid_pair(q, i, j).wait_recv()
-            return carry
-
         lax.fori_loop(0, tiles, relay, 0)
-        lax.fori_loop(0, tiles, arrive, 0)
+        ref = hid.at[chunk(q), 0 : chips * units]
+        remote(ref, ref, hp_s.at[0], hp_r.at[q], {"tp": partner}).wait_recv()
 
         def down(i, carry):
             cols = pl.ds(pl.multiple_of(i * out_tile, 128), out_tile)
@@ -316,22 +310,22 @@
     mixed = mix[...]
     ss_out[0] = row_sums(mixed * mixed)
     out_copies = [
-        remote(ss_out.at[0], ss_out.at[j], so_s.at[j], so_r.at[j], {"tp": (ti + j) % tp})
+        remote(ss_out.at[0], ss_out.at[j], so_s.at[0], so_r.at[j - 1], {"tp": (ti + j) % tp})
         for j in range(1, tp)
     ]
     for copy in out_copies:
         copy.start()
-    for copy in sent:
-        copy.wait_send()
-    for q in range(len(chunks)):
-        def drain(i, carry):
-            for j in range(1, chips):
-                hid_x(q, i, j).wait_send()
-            for j in range(chips):
-                hid_pair(q, i, j).wait_send()
-            return carry
-
-        lax.fori_loop(0, tiles, drain, 0)
+    def drain(ref, sem):
+        remote(ref, ref, sem.at[0], so_r.at[0], {"tp": partner}).wait_send()
+
+    later = pl.ds(cap, (n - 1) * cap)
+    drain(outg.at[later], d_s)
+    drain(back.at[later], r_s)
+    drain(gain.at[:, 0 : (tp - 1) * width], g_s)
+    drain(feats.at[:, 0 : (chips - 1) * width], fx_s)
+    drain(feats.at[:, 0 : chips * width], fp_s)
+    drain(hid.at[:, 0 : (chips - 1) * units], hx_s)
+    drain(hid.at[:, 0 : chips * units], hp_s)
     for copy in out_copies:
         copy.wait_recv()
     total = ss_out[0]
@@ -339,8 +333,7 @@
         total = total + ss_out[j]
     scale = wide(to_column(lax.rsqrt(total / (width * tp) + epsilon)), width)
     out_ref[...] = (mixed * scale * post_ref[...]).astype(bf16)
-    for copy in out_copies:
-        copy.wait_send()
+    drain(ss_out.at[0 : tp - 1], so_s)
 
 
 def on_device(
@@ -386,13 +379,13 @@
             pltpu.VMEM((2, rows, 128), f32),
             *[pltpu.VMEM((2, rows, count * (slots // groups)), bf16) for _, count in pieces],
             dma((3,)),
-            dma((tp,)), dma((tp,)), dma((tp,)), dma((tp,)),
-            dma((n,)), dma((n,)),
-            dma((groups, chips)), dma((groups, chips)),
-            dma((groups, chips)), dma((groups, chips)),
-            dma((steps, tiles, chips)), dma((steps, tiles, chips)),
-            dma((steps, tiles, chips)), dma((steps, tiles, chips)),
-            dma((n,)), dma((n,)),
+            dma((1,)), dma((tp - 1,)), dma((1,)), dma((tp - 1,)),
+            dma((1,)), dma((n - 1,)),
+            dma((1,)), dma((groups, chips - 1)),
+            dma((1,)), dma((groups,)),
+            dma((1,)), dma((steps, tiles, chips - 1)),
+            dma((1,)), dma((steps,)),
+            dma((1,)), dma((n - 1,)),
         ],
         compiler_params=pltpu.CompilerParams(
             collective_id=0, has_side_effects=True, vmem_limit_bytes=56 * 1024 * 1024

time: 66.3 us -> 64.5 us (0.973)
  Pallas kernels: 64.5 us -> 62.7 us
    pallas_call x1, Pallas kernels: 64.5 us -> 62.7 us  [on_device(): pl.pallas_call(functools.partial(kernel, n, tp, cap, groups, chunks, piec...]
where the time goes in v3:
time: 64.5 us; the launch traced here: 64.3 us
  Pallas kernels  62.7 us (97%)
  local copies, waits for them, and re-layouts  1.67 us (3%)
    pallas_call x1, Pallas kernels, on_device(): pl.pallas_call(functools.partial(kernel, n, tp, cap, groups, chunks, piec...  62.7 us
    unnamed x1, local copies, waits for them, and re-layouts  1.67 us

profile of v3, /device:TPU:0, one launch (start us, length us, event | category | flops | bytes accessed | tf_op | source)
XLA Modules:
  0.0 64.3 jit_solution(11520661105375984002)
XLA Ops:
  0.0 62.7 %shard_map.82 = bf16[256,512]{1,0:T(8,128)(2,1)} custom-call(bf16[256,512]{1,0:T(8,128)(2,1)} %tok_ref.1, s32[2,256]{1,0:T(2,128)} %bitcast.4, f32[2,256]{1,0:T(2,128)} %bitcast.5, f32[1,512]{1,0:T(1,128)} %bitcast.6, f32[1,512]{1,0:T(1,128)} %bitcast.7, bf16[1,2048,1024]{2,1,0:T(8,128)(2,1)} %wg_hbm.1, bf16[1,2048,1024]{2,1,0:T(8,128)(2,1)} %wu_hbm.1, ...), custom_call_target="tpu_custom_call" | custom-call | tf_op jit(solution)/shard_map/pallas_call | solution.py:361
  62.7 1.7 %copy.10 = bf16[256,512]{1,0:T(8,128)(2,1)} copy(bf16[256,512]{1,0:T(8,128)(2,1)} %shard_map.82) | data formatting | bytes 524288
